TPU v7x, 512 devices: a 4x2x32 block of a 4x8x32 slice. The times are simulated.
512 devices in a mesh: grp: 2 (over y), fs: 32 (over z), tp: 8 (over x, core).
Axes of the slice: x: 4, y: 2, z: 32, core: 2. Of those that a mesh axis runs over, the one named last changes fastest.
The devices are a block of a 4x8x32 slice.
Arguments:
- tokens: bfloat16 [20480, 2048], P(('grp', 'fs', 'tp')), parts along dimension 0, may hold values from -6 to 6
- mix_gain: bfloat16 [2048], replicated, may hold values from 0.099609375 to 1.8984375
- val_weight: bfloat16 [2048, 1024], P('fs', 'tp'), may hold values from -4 to 4
- gate_weight: bfloat16 [2048, 1024], P('fs', 'tp'), may hold values from -0.125 to 0.125
- conv_taps: bfloat16 [31, 1024], replicated, may hold values from -1 to 1
- chan_gain: bfloat16 [1024], replicated, may hold values from 0.099609375 to 1.8984375
- out_weight: bfloat16 [1024, 2048], P('tp', 'fs'), may hold values from -0.1875 to 0.1875
- mix_post_gain: bfloat16 [2048], replicated, may hold values from 0.099609375 to 1.8984375
- ffn_gain: bfloat16 [2048], replicated, may hold values from 0.099609375 to 1.8984375
- up_gate_weight: bfloat16 [2048, 5120], P('fs', 'tp'), may hold values from -0.125 to 0.125
- up_val_weight: bfloat16 [2048, 5120], P('fs', 'tp'), may hold values from -0.125 to 0.125
- ffn_taps: bfloat16 [2, 3, 5120], replicated, may hold values from -3.5 to 3.5
- down_weight: bfloat16 [5120, 2048], P('tp', 'fs'), may hold values from -0.078125 to 0.078125
- ffn_post_gain: bfloat16 [2048], replicated, may hold values from 0.099609375 to 1.8984375
Outputs:
- layer_out: bfloat16 [20480, 2048], P(('grp', 'fs', 'tp')), parts along dimension 0
There are 2 independent parts, one for each index of `grp`. A program takes and returns all parts, laid end to end along the dimension named above; an argument that names none is the same for every part. Nothing has to cross between parts.
All inputs are finite; a program needn't handle non-finite values.
Results may differ from a plain program's by a relative error of at most 0.019.
Values may be sent and summed in bfloat16 or wider, within the bound.
A program may use at most 64 MiB of HBM per device.

v0:
```python
import jax
import jax.numpy as jnp
from jax import lax
from jax.sharding import PartitionSpec as P

LEN = 64


norm_epsilon = 1e-06
chan_epsilon = 1e-05


def from_everyone(array, axis):
    copies = jnp.broadcast_to(array, (lax.axis_size(axis), *array.shape))
    return lax.all_to_all(copies, axis, split_axis=0, concat_axis=0, tiled=True)


def laid_out(blocks, dim):
    blocks = jnp.moveaxis(blocks, 0, dim)
    lengths = blocks.shape
    return blocks.reshape(*lengths[:dim], lengths[dim] * lengths[dim + 1], *lengths[dim + 2 :])


def gathered_copies(array, axis, dim):
    blocks = from_everyone(array, axis)
    return laid_out(blocks, dim)


def sent_together(arrays, axis, dim, along):
    ends, at = ([], 0)
    for a in arrays[:-1]:
        at += a.shape[along]
        ends.append(at)
    both = jnp.concatenate(arrays, axis=along)
    return tuple(jnp.split(lax.all_gather(both, axis, axis=dim, tiled=True), ends, axis=along))


def over_copies(array, axis):
    return from_everyone(array, axis).sum(axis=0)


def together(arrays, axis):
    ends = [0]
    for a in arrays:
        ends.append(ends[-1] + a.size)
    total = over_copies(jnp.concatenate([a.ravel() for a in arrays]), axis)
    return tuple((total[b:e].reshape(a.shape) for a, b, e in zip(arrays, ends, ends[1:])))


def in_blocks(array, dim, length):
    lengths = array.shape
    blocks = array.reshape(*lengths[:dim], length, lengths[dim] // length, *lengths[dim + 1 :])
    return jnp.moveaxis(blocks, dim, 0)


def summed_on_arrival(array, axis, dim):
    blocks = in_blocks(array, dim, lax.axis_size(axis))
    arrived = lax.all_to_all(blocks, axis, split_axis=0, concat_axis=0, tiled=True)
    return arrived.astype(jnp.float32).sum(axis=0)


def rms_scale(values, gain):
    inverse = lax.rsqrt(jnp.mean(values * values, axis=-1, keepdims=True) + norm_epsilon)
    return values * inverse * gain.astype(jnp.float32)


def depthwise(signal, tap_table):
    taps_count = tap_table.shape[0]
    channels = signal.shape[1]
    shaped = signal.astype(jnp.float32).reshape(signal.shape[0] // LEN, LEN, channels)
    padded = jnp.pad(shaped, ((0, 0), (taps_count - 1, 0), (0, 0)))
    tap_values = tap_table.astype(jnp.float32)
    result = jnp.zeros(shaped.shape, jnp.float32)
    for offset in range(taps_count):
        result = result + padded[:, offset : offset + LEN, :] * tap_values[offset]
    return result.reshape(signal.shape[0], channels)


def make_adder(left, pieces):
    first = jnp.dot(left, pieces[0], preferred_element_type=jnp.float32)
    second = jnp.dot(left, pieces[1], preferred_element_type=jnp.float32)
    return (first, second)


def make_rows_product(left, weight):
    return jnp.dot(left, weight, preferred_element_type=jnp.float32)


def shards(
    tokens,
    mix_gain,
    val_weight,
    gate_weight,
    conv_taps,
    chan_gain,
    out_weight,
    mix_post_gain,
    ffn_gain,
    up_gate_weight,
    up_val_weight,
    ffn_taps,
    down_weight,
    ffn_post_gain,
):
    member = lax.axis_index("tp")
    normed_own = rms_scale(tokens.astype(jnp.float32), mix_gain).astype(jnp.bfloat16)
    normed = gathered_copies(normed_own, "tp", 0)
    local_ch = val_weight.shape[1]
    values, gate_sums = make_adder(normed, sent_together((val_weight, gate_weight), "fs", 0, 1))
    glu_out = (values * jax.nn.sigmoid(gate_sums)).astype(jnp.bfloat16)
    own_taps = lax.dynamic_slice_in_dim(conv_taps, member * local_ch, local_ch, 1)
    conv_out = depthwise(glu_out, own_taps)
    totals, squares = together(
        (jnp.sum(conv_out, axis=1), jnp.sum(conv_out * conv_out, axis=1)), "tp"
    )
    all_channels = chan_gain.shape[0]
    chan_mean = totals[:, None] / all_channels
    chan_var = squares[:, None] / all_channels - chan_mean * chan_mean
    own_gain = lax.dynamic_slice_in_dim(chan_gain, member * local_ch, local_ch, 0).astype(
        jnp.float32
    )
    activated = jax.nn.silu((conv_out - chan_mean) * lax.rsqrt(chan_var + chan_epsilon) * own_gain)
    activated = activated.astype(jnp.bfloat16)
    out_full = lax.all_gather(out_weight, "fs", axis=1, tiled=True)
    mixed_sum = summed_on_arrival(
        make_rows_product(activated, out_full).astype(jnp.bfloat16), "tp", 0
    )
    residual = (tokens.astype(jnp.float32) + rms_scale(mixed_sum, mix_post_gain)).astype(
        jnp.bfloat16
    )
    normed_share = rms_scale(residual.astype(jnp.float32), ffn_gain).astype(jnp.bfloat16)
    normed_ffn = gathered_copies(normed_share, "tp", 0)
    local_ff = up_gate_weight.shape[1]
    own_ffn_taps = lax.dynamic_slice_in_dim(ffn_taps, member * local_ff, local_ff, 2)
    gate_full, val_full = sent_together((up_gate_weight, up_val_weight), "fs", 0, 1)
    up_gate = jnp.dot(normed_ffn, gate_full, preferred_element_type=jnp.float32).astype(
        jnp.bfloat16
    )
    up_val = jnp.dot(normed_ffn, val_full, preferred_element_type=jnp.float32).astype(jnp.bfloat16)
    gate_conv = depthwise(up_gate, own_ffn_taps[0])
    val_conv = depthwise(up_val, own_ffn_taps[1])
    hidden = (jax.nn.gelu(gate_conv, approximate=True) * val_conv).astype(jnp.bfloat16)
    down_full = lax.all_gather(down_weight, "fs", axis=1, tiled=True)
    ffn_sum = summed_on_arrival(make_rows_product(hidden, down_full).astype(jnp.bfloat16), "tp", 0)
    return (residual.astype(jnp.float32) + rms_scale(ffn_sum, ffn_post_gain)).astype(jnp.bfloat16)


def solution(mesh):
    return jax.shard_map(
        shards,
        mesh=mesh,
        in_specs=(
            P(("grp", "fs", "tp"), None),
            P(),
            P("fs", "tp"),
            P("fs", "tp"),
            P(),
            P(),
            P("tp", "fs"),
            P(),
            P(),
            P("fs", "tp"),
            P("fs", "tp"),
            P(),
            P("tp", "fs"),
            P(),
        ),
        out_specs=P(("grp", "fs", "tp"), None),
        check_vma=False,
    )
```

profile of v0, /device:TPU:33, one launch (start us, length us, event | category | flops | bytes accessed | tf_op | source)
XLA Modules:
  0.0 472.4 jit_solution(905065115232511449)
XLA Ops:
  6.6 1.3 pad_maximum_fusion.1
  8.0 1.6 pad_maximum_fusion
  10.4 1.1 fusion.33
  11.5 1.0 fusion.35
  12.5 1.3 broadcast_in_dim.6
  13.7 45.0 %all-to-all-start = ((bf16[8,40,2048]{2,1,0:T(8,128)(2,1)}), bf16[8,40,2048]{2,1,0:T(8,128)(2,1)S(1)}, u32[]{:S(2)}, u32[]{:S(2)}) async-start(bf16[8,40,2048]{2,1,0:T(8,128)(2,1)} %broadcast_in_dim.6), calls=%async_computation | async-start | bytes 2621440 | tf_op jit(solution)/shard_map/all_to_all | solution.py:15
  59.5 46.8 %all_gather.13 = bf16[128,2048]{0,1:T(8,128)(2,1)S(1)} all-gather(bf16[128,64]{0,1:T(8,128)(2,1)S(1)} %copy-done.2), channel_id=1, replica_groups=mesh['grp'=2,'fs'=32,'tp'=8] {'fs'}, dimensions={1}, use_global_device_ids=true | all-gather | bytes 540672 | tf_op jit(solution)/shard_map/all_gather | solution.py:124
  106.3 43.0 %all-gather.4.cloned.1.call-done = bf16[2048,256]{1,0:T(8,128)(2,1)} async-done(((bf16[64,256]{1,0:T(8,128)(2,1)}), bf16[2048,256]{1,0:T(8,128)(2,1)}) %all-gather.4.cloned.1.call-update) | async-done | bytes 1048592 | tf_op jit(solution)/shard_map/all_gather | solution.py:35
  149.3 1.6 fusion.12
  153.0 25.4 %all-to-all-start.1 = ((f32[8,1,640]{2,1,0:T(1,128)}), f32[8,1,640]{2,1,0:T(1,128)S(1)}, u32[]{:S(2)}, u32[]{:S(2)}) async-start(f32[8,1,640]{2,1,0:T(1,128)} %broadcast_in_dim.7), calls=%async_computation.1 | async-start | bytes 40960 | tf_op jit(solution)/shard_map/all_to_all | solution.py:15
  179.2 3.9 all-to-all-done.1
  183.4 1.7 convolution_convert_fusion
  185.1 4.3 all-to-all-start.2
  190.2 17.1 %all-to-all-done.2 = bf16[8,40,2048]{2,1,0:T(8,128)(2,1)S(1)} async-done(((bf16[8,40,2048]{2,1,0:T(8,128)(2,1)}), bf16[8,40,2048]{2,1,0:T(8,128)(2,1)S(1)}, u32[]{:S(2)}, u32[]{:S(2)}) %all-to-all-start.2) | async-done | bytes 1310752 | tf_op jit(solution)/shard_map/all_to_all | solution.py:58
  208.0 1.3 broadcast_in_dim.8
  209.3 4.4 all-to-all-start.3
  214.7 17.0 %all-to-all-done.3 = bf16[8,40,2048]{2,1,0:T(8,128)(2,1)S(1)} async-done(((bf16[8,40,2048]{2,1,0:T(8,128)(2,1)}), bf16[8,40,2048]{2,1,0:T(8,128)(2,1)S(1)}, u32[]{:S(2)}, u32[]{:S(2)}) %all-to-all-start.3) | async-done | bytes 1310752 | tf_op jit(solution)/shard_map/all_to_all | solution.py:15
  231.6 55.6 %all-gather.6.cloned.1.call-done = bf16[2048,1280]{1,0:T(8,128)(2,1)} async-done(((bf16[64,1280]{1,0:T(8,128)(2,1)}), bf16[2048,1280]{1,0:T(8,128)(2,1)}) %all-gather.6.cloned.1.call-update) | async-done | bytes 5242896 | tf_op jit(solution)/shard_map/all_gather | solution.py:35
  287.2 3.1 fusion.4
  290.5 1.2 fusion.7
  292.5 124.9 %all-gather.8.cloned.1.call-done = bf16[640,2048]{0,1:T(8,128)(2,1)} async-done(((bf16[640,64]{0,1:T(8,128)(2,1)}), bf16[640,2048]{0,1:T(8,128)(2,1)}) %all-gather.8.cloned.1.call-update) | async-done | bytes 2621456 | tf_op jit(solution)/shard_map/all_gather | solution.py:143
  417.5 4.0 convolution_convert_fusion.1
  421.5 25.5 %all-to-all-start.4 = ((bf16[8,40,2048]{2,1,0:T(8,128)(2,1)}), bf16[8,40,2048]{2,1,0:T(8,128)(2,1)S(1)}, u32[]{:S(2)}, u32[]{:S(2)}) async-start(bf16[8,40,2048]{2,1,0:T(8,128)(2,1)} %bitcast.43), calls=%async_computation.4 | async-start | bytes 2621440 | tf_op jit(solution)/shard_map/all_to_all | solution.py:58
  447.0 17.8 %all-to-all-done.4 = bf16[8,40,2048]{2,1,0:T(8,128)(2,1)S(1)} async-done(((bf16[8,40,2048]{2,1,0:T(8,128)(2,1)}), bf16[8,40,2048]{2,1,0:T(8,128)(2,1)S(1)}, u32[]{:S(2)}, u32[]{:S(2)}) %all-to-all-start.4) | async-done | bytes 1310752 | tf_op jit(solution)/shard_map/all_to_all | solution.py:58
  (57 shorter events, 9.1 us)
Async XLA Ops:
  6.5 142.8 %all-gather.4.cloned.1.call-start = ((), (), s32[]{:S(2)}) async-start(), calls=%async_computation.5 | async-start | bytes 1081344 | tf_op jit(solution)/shard_map/all_gather | solution.py:35
  8.0 279.3 %all-gather.6.cloned.1.call-start = ((), (), s32[]{:S(2)}) async-start(), calls=%async_computation.6 | async-start | bytes 5406720 | tf_op jit(solution)/shard_map/all_gather | solution.py:35
  13.7 45.8 %copy-start.2 = (bf16[128,64]{0,1:T(8,128)(2,1)S(1)}, bf16[128,64]{0,1:T(8,128)(2,1)}, u32[]{:S(2)}) copy-start(bf16[128,64]{0,1:T(8,128)(2,1)} %param.20) | copy-start | bytes 49156
  13.7 92.6 %all-to-all-start = ((bf16[8,40,2048]{2,1,0:T(8,128)(2,1)}), bf16[8,40,2048]{2,1,0:T(8,128)(2,1)S(1)}, u32[]{:S(2)}, u32[]{:S(2)}) async-start(bf16[8,40,2048]{2,1,0:T(8,128)(2,1)} %broadcast_in_dim.6), calls=%async_computation | async-start | bytes 2621440 | tf_op jit(solution)/shard_map/all_to_all | solution.py:15
  149.3 1.7 copy-start.1
  153.0 30.1 %all-to-all-start.1 = ((f32[8,1,640]{2,1,0:T(1,128)}), f32[8,1,640]{2,1,0:T(1,128)S(1)}, u32[]{:S(2)}, u32[]{:S(2)}) async-start(f32[8,1,640]{2,1,0:T(1,128)} %broadcast_in_dim.7), calls=%async_computation.1 | async-start | bytes 40960 | tf_op jit(solution)/shard_map/all_to_all | solution.py:15
  185.1 5.1 %copy-start.3 = (bf16[2048]{0:T(1024)(128)(2,1)S(1)}, bf16[2048]{0:T(1024)(128)(2,1)}, u32[]{:S(2)}) copy-start(bf16[2048]{0:T(1024)(128)(2,1)} %param.21) | copy-start | bytes 12292
  185.1 5.1 %copy-start.4 = (bf16[2048]{0:T(1024)(128)(2,1)S(1)}, bf16[2048]{0:T(1024)(128)(2,1)}, u32[]{:S(2)}) copy-start(bf16[2048]{0:T(1024)(128)(2,1)} %param.22) | copy-start | bytes 12292
  185.1 22.2 %all-to-all-start.2 = ((bf16[8,40,2048]{2,1,0:T(8,128)(2,1)}), bf16[8,40,2048]{2,1,0:T(8,128)(2,1)S(1)}, u32[]{:S(2)}, u32[]{:S(2)}) async-start(bf16[8,40,2048]{2,1,0:T(8,128)(2,1)} %bitcast.35), calls=%async_computation.2 | async-start | bytes 2621440 | tf_op jit(solution)/shard_map/all_to_all | solution.py:58
  189.4 18.2 %copy-start = (bf16[40,2048]{1,0:T(8,128)(2,1)S(1)}, bf16[40,2048]{1,0:T(8,128)(2,1)}, u32[]{:S(2)}) copy-start(bf16[40,2048]{1,0:T(8,128)(2,1)} %param.14) | copy-start | bytes 491524
  189.4 228.1 %all-gather.8.cloned.1.call-start = ((), (), s32[]{:S(2)}) async-start(), calls=%async_computation.7 | async-start | bytes 2703360 | tf_op jit(solution)/shard_map/all_gather | solution.py:143
  209.3 22.3 %all-to-all-start.3 = ((bf16[8,40,2048]{2,1,0:T(8,128)(2,1)}), bf16[8,40,2048]{2,1,0:T(8,128)(2,1)S(1)}, u32[]{:S(2)}, u32[]{:S(2)}) async-start(bf16[8,40,2048]{2,1,0:T(8,128)(2,1)} %broadcast_in_dim.8), calls=%async_computation.3 | async-start | bytes 2621440 | tf_op jit(solution)/shard_map/all_to_all | solution.py:15
  287.2 3.3 copy-start.6
  421.5 25.5 %copy-start.5 = (bf16[2048]{0:T(1024)(128)(2,1)S(1)}, bf16[2048]{0:T(1024)(128)(2,1)}, u32[]{:S(2)}) copy-start(bf16[2048]{0:T(1024)(128)(2,1)} %param.27) | copy-start | bytes 12292
  421.5 43.3 %all-to-all-start.4 = ((bf16[8,40,2048]{2,1,0:T(8,128)(2,1)}), bf16[8,40,2048]{2,1,0:T(8,128)(2,1)S(1)}, u32[]{:S(2)}, u32[]{:S(2)}) async-start(bf16[8,40,2048]{2,1,0:T(8,128)(2,1)} %bitcast.43), calls=%async_computation.4 | async-start | bytes 2621440 | tf_op jit(solution)/shard_map/all_to_all | solution.py:58
Sparse Core Ops, SparseCore 0:
  9.4 139.8 all-gather.3
  151.4 135.7 all-gather.5
  289.3 128.1 all-gather.7
where the time goes:
time: 473 us; the launch traced here: 472 us
  waiting for transfers between devices  280 us (59%)
  starting transfers between devices  105 us (22%)
  blocking collectives  46.8 us (10%)
  between operations  13.3 us (3%)
  matrix products  12.1 us (3%)
  other arithmetic  11.8 us (2%)
    all_gather x1, waiting for transfers between devices, shards(): down_full = lax.all_gather(down_weight, 'fs', axis=1, tiled=True)  125 us
    all_gather x2, waiting for transfers between devices, sent_together(): lax.all_gather(both, axis, axis=dim, tiled=True)  98.6 us
    all_to_all x3, starting transfers between devices, from_everyone(): return lax.all_to_all(copies, axis, split_axis=0, concat_axis=0, tiled=True)  74.9 us
    all_gather x1, blocking collectives, shards(): out_full = lax.all_gather(out_weight, 'fs', axis=1, tiled=True)  46.8 us
    all_to_all x2, waiting for transfers between devices, summed_on_arrival(): lax.all_to_all(blocks, axis, split_axis=0, concat_axis=0, tiled=True)  34.8 us
    all_to_all x2, starting transfers between devices, summed_on_arrival(): lax.all_to_all(blocks, axis, split_axis=0, concat_axis=0, tiled=True)  29.8 us
    all_to_all x3, waiting for transfers between devices, from_everyone(): return lax.all_to_all(copies, axis, split_axis=0, concat_axis=0, tiled=True)  20.9 us
  transfers between devices with their start and end apart: 8, of which 7 were waited for; matrix products, arithmetic and copies ran while one was open for 4% of the time, Pallas kernels for 0%

commit v1 on v0

v1 whole, which is shorter than its diff:
```python
import functools

import jax
import jax.numpy as jnp
from jax import lax
from jax.experimental import pallas as pl
from jax.experimental.pallas import tpu as pltpu
from jax.sharding import PartitionSpec as P

LEN = 64
MESH = pl.DeviceIdType.MESH
F32 = jnp.float32
BF16 = jnp.bfloat16
NT = (((1,), (1,)), ((), ()))

norm_epsilon = 1e-06
chan_epsilon = 1e-05

LANES = 128
PAIR = 2 * LANES
PAD_ROWS = 32
FPAD = 8


class Ring:
    def __init__(self, n, me, block, streams, offsets, send_sem, recv_sem):
        self.n, self.me, self.block = n, me, block
        self.streams, self.offsets = streams, offsets
        self.send_sem, self.recv_sem = send_sem, recv_sem
        self.steps = (n // 2, (n - 1) - n // 2)
        self.peers = (lax.rem(me + 1, n), lax.rem(me + n - 1, n))
        self.at = 0
        self.last = max(offsets) + self.steps[0]

    def copy(self, j, way, owner, step):
        ref = self.streams[j](owner)
        return pltpu.make_async_remote_copy(
            src_ref=ref,
            dst_ref=ref,
            send_sem=self.send_sem.at[j, way],
            recv_sem=self.recv_sem.at[j, way, step],
            device_id={"fs": self.peers[way]},
            device_id_type=MESH,
        )

    def owner(self, way, step):
        shift = (self.n - step) if way == 0 else step
        return lax.rem(self.me + shift, self.n)

    def arrived(self, j, way, step):
        self.copy(j, way, self.owner(way, step + 1), step).wait_recv()

    def slot(self, k, active):
        for j, first in active:
            for way in (0, 1):
                step = k - self.offsets[j]
                if first:
                    if self.steps[way] > 0:
                        self.copy(j, way, self.me, 0).start()
                    continue

                def go(j=j, way=way, step=step):
                    self.arrived(j, way, step - 1)
                    self.copy(j, way, self.owner(way, step), step).start()

                if way == 0 or isinstance(step, int):
                    if step < self.steps[way] if isinstance(step, int) else True:
                        go()
                else:
                    pl.when(step < self.steps[way])(go)

    def active(self, k):
        return tuple(
            (j, k == off)
            for j, off in enumerate(self.offsets)
            if off <= k < off + self.steps[0]
        )

    def short(self, k):
        return tuple(k - off >= self.steps[1] for off in self.offsets)

    def pump_to(self, upto):
        upto = min(upto, self.last)
        while self.at < upto:
            key = (self.active(self.at), self.short(self.at))
            end = self.at
            while end < upto and (self.active(end), self.short(end)) == key:
                end += 1
            steady = end - self.at > 1 and not any(f for _, f in key[0])
            if steady and not any(key[1][j] for j, _ in key[0]):
                lax.fori_loop(
                    self.at, end, lambda k, z, key=key: (self.slot_loop(k, key[0]), z)[1], 0
                )
                self.at = end
            else:
                self.slot(self.at, self.active(self.at))
                self.at += 1

    def slot_loop(self, k, active):
        for j, _ in active:
            for way in (0, 1):
                step = k - self.offsets[j]
                self.arrived(j, way, step - 1)
                self.copy(j, way, self.owner(way, step), step).start()

    def finish(self, js):
        self.pump_to(max(self.offsets[j] + self.steps[0] for j in js))
        for j in js:
            for way in (0, 1):
                if self.steps[way] > 0:
                    self.arrived(j, way, self.steps[way] - 1)

    def drain(self, wholes):
        for j, whole in enumerate(wholes):
            for way in (0, 1):
                if self.steps[way] > 0:
                    ref = whole(self.steps[way])
                    pltpu.make_async_copy(ref, ref, self.send_sem.at[j, way]).wait()


def layer_kernel(
    n,
    tp,
    tokens,
    mix_gain,
    val_h,
    gate_h,
    conv_taps,
    chan_gain,
    out_w,
    mix_post_gain,
    ffn_gain,
    up_gate_h,
    up_val_h,
    ffn_taps,
    down_w,
    ffn_post_gain,
    out,
    vg,
    outt,
    up,
    downt,
    xg,
    lhs,
    prod,
    din,
    psum,
    opp,
    near,
    comb,
    fin,
    got,
    cbuf,
    conv,
    stats,
    resid,
    fbuf,
    hidden,
    load_sem,
    zsend,
    zrecv,
    xsend,
    xrecv,
    ssend,
    srecv,
):
    rows, width = tokens.shape
    half, quarter = width // 2, width // 4
    block = width // n
    group_rows = rows * tp
    chip_rows = 2 * rows
    chips = tp // 2
    pieces = up_gate_h.shape[1] // LANES
    f = lax.axis_index("fs")
    t = lax.axis_index("tp")
    x, c = t // 2, lax.rem(t, 2)
    partner = t + 1 - 2 * c
    xr, xl, xo = (lax.rem(x + s, chips) for s in (1, chips - 1, 2))
    tr, tl, to = (2 * v + c for v in (xr, xl, xo))
    odd = c == 1

    mine = pl.ds(pl.multiple_of(f * block, block), block)
    loads = [
        pltpu.make_async_copy(val_h, vg.at[mine, pl.ds(0, LANES)], load_sem.at[0]),
        pltpu.make_async_copy(gate_h, vg.at[mine, pl.ds(LANES, LANES)], load_sem.at[1]),
    ]
    for j in range(pieces):
        columns = pl.ds(j * LANES, LANES)
        loads.append(
            pltpu.make_async_copy(
                up_gate_h.at[:, columns], up.at[j, mine, pl.ds(0, LANES)], load_sem.at[2 + 2 * j]
            )
        )
        loads.append(
            pltpu.make_async_copy(
                up_val_h.at[:, columns], up.at[j, mine, pl.ds(LANES, LANES)], load_sem.at[3 + 2 * j]
            )
        )
    for load in loads:
        load.start()

    barrier = pltpu.get_barrier_semaphore()
    for z in (lax.rem(f + 1, n), lax.rem(f + n - 1, n)):
        pl.semaphore_signal(barrier, inc=1, device_id={"fs": z}, device_id_type=MESH)
    for d in range(1, tp):
        pl.semaphore_signal(
            barrier, inc=1, device_id={"tp": lax.rem(t + d, tp)}, device_id_type=MESH
        )

    eye = jnp.where(
        lax.broadcasted_iota(jnp.int32, (block, block), 0)
        == lax.broadcasted_iota(jnp.int32, (block, block), 1),
        1.0,
        0.0,
    ).astype(BF16)
    outt[mine, :] = lax.dot_general(eye, out_w[...], NT, preferred_element_type=F32).astype(BF16)
    downt[mine, :] = lax.dot_general(eye, down_w[...], NT, preferred_element_type=F32).astype(BF16)

    def zview(buffer, owner):
        return buffer.at[pl.ds(pl.multiple_of(owner * block, block), block), :]

    def down_view(part, owner):
        size = block // 2
        start = pl.multiple_of(owner * block + part * size, size)
        return downt.at[pl.ds(start, size), :]

    streams = [functools.partial(zview, vg), functools.partial(zview, outt)]
    streams += [functools.partial(zview, up.at[j]) for j in range(pieces)]
    streams += [functools.partial(down_view, part) for part in (0, 1)]
    steps = n // 2
    ups = list(range(2, 2 + pieces))
    downs = [2 + pieces, 3 + pieces]
    offsets = [0, 0] + [0 if j < 2 else steps for j in range(pieces)] + [2 * steps] * 2
    ring = Ring(n, f, block, streams, offsets, zsend, zrecv)

    def put_normed(u, left, right, gain):
        scale = lax.rsqrt(
            (
                jnp.sum(left * left, axis=1, keepdims=True)
                + jnp.sum(right * right, axis=1, keepdims=True)
            )
            / width
            + norm_epsilon
        )
        pad = jnp.zeros((8, half), F32)
        for at, part in ((0, left), (half, right)):
            value = part * scale * gain[:, at : at + half].astype(F32)
            low = jnp.concatenate([value, pad], axis=0)
            high = jnp.concatenate([pad, value], axis=0)
            xg[u, t, :, at : at + half] = jnp.where(odd, high, low).astype(BF16)

    def x_copy(u, sem, src, dst, where):
        return pltpu.make_async_remote_copy(
            src_ref=src,
            dst_ref=dst,
            send_sem=xsend.at[u, sem],
            recv_sem=xrecv.at[u, sem],
            device_id={"tp": where},
            device_id_type=MESH,
        )

    first, second = pl.ds(0, half), pl.ds(half, half)

    def spread(u, slots):
        own, from_l, from_r = xg.at[u, t], xg.at[u, tl], xg.at[u, tr]
        opp_l, opp_r = xg.at[u, to, :, first], xg.at[u, to, :, second]
        sent = [
            x_copy(u, 1, own, own, tr),
            x_copy(u, 2, own, own, tl),
            x_copy(u, 0, own, own, partner),
        ]
        for copy in sent:
            copy.start()
        ring.pump_to(slots[0])
        more = []
        x_copy(u, 1, from_l, from_l, tr).wait_recv()
        more.append(x_copy(u, 3, from_l.at[:, first], from_l.at[:, first], tr))
        more.append(x_copy(u, 5, from_l, from_l, partner))
        more[0].start()
        x_copy(u, 2, from_r, from_r, tl).wait_recv()
        more.append(x_copy(u, 4, from_r.at[:, second], from_r.at[:, second], tl))
        more.append(x_copy(u, 6, from_r, from_r, partner))
        for copy in more[2:3] + more[1:2] + more[3:4]:
            copy.start()
        sent += more
        ring.pump_to(slots[1])
        x_copy(u, 3, opp_l, opp_l, tr).wait_recv()
        last = [x_copy(u, 7, opp_l, opp_l, partner)]
        last[0].start()
        x_copy(u, 4, opp_r, opp_r, tl).wait_recv()
        last.append(x_copy(u, 8, opp_r, opp_r, partner))
        last[1].start()
        sent += last
        ring.pump_to(slots[2])
        other = 1 - 2 * c
        for sem, ref in (
            (0, xg.at[u, partner]),
            (5, xg.at[u, tl + other]),
            (6, xg.at[u, tr + other]),
            (7, xg.at[u, to + other, :, first]),
            (8, xg.at[u, to + other, :, second]),
        ):
            x_copy(u, sem, ref, ref, partner).wait_recv()
        for chip in range(chips):
            a, b, base = xg.at[u, 2 * chip], xg.at[u, 2 * chip + 1], chip * chip_rows
            lhs[base : base + 32, :] = a[0:32, :]
            lhs[base + 32 : base + 48, :] = a[32:48, :] + b[0:16, :]
            lhs[base + 48 : base + 80, :] = b[16:48, :]
        return sent

    def chip_rows_at(v):
        return pl.ds(pl.multiple_of(v * chip_rows, 16), chip_rows)

    q0, q1 = pl.ds(0, quarter), pl.ds(quarter, quarter)

    def collect(u, slots):
        mine_h = pl.ds(pl.multiple_of(c * half, half), half)
        other_h = pl.ds(pl.multiple_of((1 - c) * half, half), half)
        sent = [x_copy(u, 9, prod.at[u, :, other_h], din.at[u], partner)]
        sent[0].start()
        ring.pump_to(slots[0])
        x_copy(u, 9, prod.at[u, :, other_h], din.at[u], partner).wait_recv()
        psum[u, :, :] = (
            prod[u, :, mine_h].astype(F32) + din[u, :, :].astype(F32)
        ).astype(BF16)
        plan = [
            (10, psum.at[u, chip_rows_at(xo), q0], opp.at[u, 0], tr),
            (11, psum.at[u, chip_rows_at(xo), q1], opp.at[u, 1], tl),
            (12, psum.at[u, chip_rows_at(xr), q1], near.at[u, 0, 1], tr),
            (13, psum.at[u, chip_rows_at(xl), q0], near.at[u, 1, 0], tl),
        ]
        for item in plan:
            copy = x_copy(u, *item)
            copy.start()
            sent.append(copy)
        ring.pump_to(slots[1])
        for way, sem, v, q, where in ((0, 10, xr, q0, tr), (1, 11, xl, q1, tl)):
            x_copy(u, sem, psum.at[u, chip_rows_at(xo), q], opp.at[u, way], where).wait_recv()
            comb[u, way, :, :] = (
                psum[u, chip_rows_at(v), q].astype(F32) + opp[u, way, :, :].astype(F32)
            ).astype(BF16)
            copy = x_copy(u, 14 + way, comb.at[u, way], near.at[u, way, way], where)
            copy.start()
            sent.append(copy)
        ring.pump_to(slots[2])
        for sem, way, part, where in ((12, 0, 1, tr), (13, 1, 0, tl), (14, 0, 0, tr), (15, 1, 1, tl)):
            x_copy(u, sem, comb.at[u, way], near.at[u, way, part], where).wait_recv()
        for part, q in ((0, q0), (1, q1)):
            fin[u, :, q] = (
                psum[u, chip_rows_at(x), q].astype(F32)
                + near[u, 0, part, :, :].astype(F32)
                + near[u, 1, part, :, :].astype(F32)
            )
        mine_r = pl.ds(pl.multiple_of(c * rows, 8), rows)
        other_r = pl.ds(pl.multiple_of((1 - c) * rows, 8), rows)
        copy = x_copy(u, 16, fin.at[u, other_r, :], got.at[u], partner)
        copy.start()
        sent.append(copy)
        ring.pump_to(slots[3])
        copy.wait_recv()
        here, there = fin[u, mine_r, :], got[u, :, :]
        return jnp.where(odd, there, here), jnp.where(odd, here, there), sent

    left = tokens[:, 0:half].astype(F32)
    right = tokens[:, half:width].astype(F32)
    put_normed(0, left, right, mix_gain)
    pl.semaphore_wait(barrier, tp + 1)
    for load in loads:
        load.wait()
    ring.pump_to(1)
    sent = spread(0, (2, 4, 5))

    ring.finish([0])
    both = jnp.dot(lhs[...], vg[...], preferred_element_type=F32)
    glu = (both[:, 0:LANES] * jax.nn.sigmoid(both[:, LANES:PAIR])).astype(BF16).astype(F32)
    segments = group_rows // LEN
    taps_n = conv_taps.shape[0]
    cbuf[:, 0:PAD_ROWS, :] = jnp.zeros((segments, PAD_ROWS, LANES), F32)
    for s in range(segments):
        cbuf[s, PAD_ROWS:, :] = glu[s * LEN : (s + 1) * LEN, :]
    my_ch = pl.ds(pl.multiple_of(t * LANES, LANES), LANES)
    taps = conv_taps[:, my_ch].astype(F32)

    def convolve(s, z):
        total = jnp.zeros((LEN, LANES), F32)
        for k in range(taps_n):
            at = PAD_ROWS - (taps_n - 1) + k
            total = total + cbuf[s, at : at + LEN, :] * taps[k : k + 1, :]
        conv[pl.ds(pl.multiple_of(s * LEN, LEN), LEN), :] = total
        return z

    lax.fori_loop(0, segments, convolve, 0)
    conv_out = conv[...]
    ones = jnp.ones((8, LANES), F32)
    high = lax.Precision.HIGHEST
    sums = lax.dot_general(ones, conv_out, NT, precision=high, preferred_element_type=F32)
    squares = lax.dot_general(
        ones, conv_out * conv_out, NT, precision=high, preferred_element_type=F32
    )
    pick = lax.broadcasted_iota(jnp.int32, (8, group_rows), 0) < 4
    stats[t, :, 0:group_rows] = jnp.where(pick, sums, squares)

    def stat_copy(d):
        return pltpu.make_async_remote_copy(
            src_ref=stats.at[t],
            dst_ref=stats.at[t],
            send_sem=ssend.at[d - 1],
            recv_sem=srecv.at[d - 1],
            device_id={"tp": lax.rem(t + d, tp)},
            device_id_type=MESH,
        )

    stat_copies = [stat_copy(d) for d in range(1, tp)]
    for copy in stat_copies:
        copy.start()
    ring.finish([1])
    for d in range(1, tp):
        source = lax.rem(t + tp - d, tp)
        pltpu.make_async_remote_copy(
            src_ref=stats.at[source],
            dst_ref=stats.at[source],
            send_sem=ssend.at[d - 1],
            recv_sem=srecv.at[d - 1],
            device_id={"tp": source},
            device_id_type=MESH,
        ).wait_recv()
    channels = chan_gain.shape[1]
    both_stats = jnp.sum(stats[:, :, 0:group_rows], axis=0) / channels
    flipped = jnp.transpose(
        jnp.concatenate([both_stats] + [jnp.zeros((8, group_rows), F32)] * 15, axis=0)
    )
    mean, square = flipped[:, 0:1], flipped[:, 4:5]
    scale = lax.rsqrt(square - mean * mean + chan_epsilon)
    normal = (conv_out - mean) * scale * chan_gain[:, my_ch].astype(F32)
    activated = (normal * jax.nn.sigmoid(normal)).astype(BF16)
    wide = min(512, width)
    for j in range(width // wide):
        prod[0, :, j * wide : (j + 1) * wide] = lax.dot_general(
            activated, outt[j * wide : (j + 1) * wide, :], NT, preferred_element_type=F32
        ).astype(BF16)

    base = ring.at
    left_sum, right_sum, more = collect(0, (base + 1, base + 2, base + 4, base + 5))
    sent += more

    def rms(a, b, gain):
        scale = lax.rsqrt(
            (jnp.sum(a * a, axis=1, keepdims=True) + jnp.sum(b * b, axis=1, keepdims=True)) / width
            + norm_epsilon
        )
        return (
            a * scale * gain[:, 0:half].astype(F32),
            b * scale * gain[:, half:width].astype(F32),
        )

    a, b = rms(left_sum, right_sum, mix_post_gain)
    res_a = (tokens[:, 0:half].astype(F32) + a).astype(BF16)
    res_b = (tokens[:, half:width].astype(F32) + b).astype(BF16)
    resid[:, 0:half] = res_a.astype(F32)
    resid[:, half:width] = res_b.astype(F32)
    put_normed(1, res_a.astype(F32), res_b.astype(F32), ffn_gain)
    base = ring.at
    sent += spread(1, (base + 1, base + 2, base + 3))

    fbuf[:, 0:FPAD, :] = jnp.zeros((segments, FPAD, PAIR), F32)
    ftaps_n = ffn_taps.shape[1]

    def feed(j):
        pair = jnp.dot(lhs[...], up[j], preferred_element_type=F32).astype(BF16).astype(F32)
        for s in range(segments):
            fbuf[s, FPAD:, :] = pair[s * LEN : (s + 1) * LEN, :]
        here = pl.ds(pl.multiple_of(t * (pieces * LANES) + j * LANES, LANES), LANES)
        gate_taps = ffn_taps[0, :, here].astype(F32)
        val_taps = ffn_taps[1, :, here].astype(F32)
        for s in range(segments):
            gate = jnp.zeros((LEN, LANES), F32)
            val = jnp.zeros((LEN, LANES), F32)
            for k in range(ftaps_n):
                at = FPAD - (ftaps_n - 1) + k
                gate = gate + fbuf[s, at : at + LEN, 0:LANES] * gate_taps[k : k + 1, :]
                val = val + fbuf[s, at : at + LEN, LANES:PAIR] * val_taps[k : k + 1, :]
            hidden[j, s * LEN : (s + 1) * LEN, :] = (
                jax.nn.gelu(gate, approximate=True) * val
            ).astype(BF16)

    early = [j for j in range(pieces) if offsets[2 + j] == 0]
    late = [j for j in range(pieces) if offsets[2 + j] > 0]
    ring.finish([2 + j for j in early])
    for j in early:
        feed(j)
        ring.pump_to(ring.at + 1)
    ring.finish([2 + j for j in late])
    for j in late:
        feed(j)
        ring.pump_to(ring.at + 2)
    ring.finish(downs)

    def contract(j, z):
        columns = pl.ds(pl.multiple_of(j * PAIR, PAIR), PAIR)
        units = jnp.concatenate([hidden[i] for i in range(pieces)], axis=1)
        prod[1, :, columns] = lax.dot_general(
            units, downt[columns, :], NT, preferred_element_type=F32
        ).astype(BF16)
        return z

    lax.fori_loop(0, width // PAIR, contract, 0)
    left_sum, right_sum, more = collect(1, (0, 0, 0, 0))
    sent += more
    a, b = rms(left_sum, right_sum, ffn_post_gain)
    out[:, 0:half] = (resid[:, 0:half] + a).astype(BF16)
    out[:, half:width] = (resid[:, half:width] + b).astype(BF16)

    for copy in sent + stat_copies:
        copy.wait_send()

    def whole_of(buffer, size, count):
        return buffer.at[pl.ds(0, count * size), :]

    wholes = [functools.partial(whole_of, vg, block), functools.partial(whole_of, outt, block)]
    wholes += [functools.partial(whole_of, up.at[j], block) for j in range(pieces)]
    wholes += [functools.partial(whole_of, downt, block // 2)] * 2
    ring.drain(wholes)


def shards(*args):
    (tokens, mix_gain, val_weight, _, conv_taps, chan_gain, out_weight) = args[:7]
    up_weight, down_weight = args[9], args[12]
    n, tp = lax.axis_size("fs"), lax.axis_size("tp")
    rows, width = tokens.shape
    block = width // n
    half, quarter = width // 2, width // 4
    group_rows, chip_rows = rows * tp, 2 * rows
    segments = group_rows // LEN
    pieces = up_weight.shape[1] // LANES
    streams = 4 + pieces
    steps = n // 2
    args = [a.reshape(1, -1) if a.ndim == 1 else a for a in args]
    vmem = pl.BlockSpec(memory_space=pltpu.VMEM)
    hbm = pl.BlockSpec(memory_space=pltpu.HBM)
    dma = pltpu.SemaphoreType.DMA
    return pl.pallas_call(
        functools.partial(layer_kernel, n, tp),
        out_shape=jax.ShapeDtypeStruct((rows, width), BF16),
        in_specs=[hbm if i in (2, 3, 9, 10) else vmem for i in range(len(args))],
        out_specs=vmem,
        scratch_shapes=[
            pltpu.VMEM((width, PAIR), BF16),
            pltpu.VMEM((width, LANES), BF16),
            pltpu.VMEM((pieces, width, PAIR), BF16),
            pltpu.VMEM((width, pieces * LANES), BF16),
            pltpu.VMEM((2, tp, rows + 8, width), BF16),
            pltpu.VMEM((group_rows, width), BF16),
            pltpu.VMEM((2, group_rows, width), BF16),
            pltpu.VMEM((2, group_rows, half), BF16),
            pltpu.VMEM((2, group_rows, half), BF16),
            pltpu.VMEM((2, 2, chip_rows, quarter), BF16),
            pltpu.VMEM((2, 2, 2, chip_rows, quarter), BF16),
            pltpu.VMEM((2, 2, chip_rows, quarter), BF16),
            pltpu.VMEM((2, chip_rows, half), F32),
            pltpu.VMEM((2, rows, half), F32),
            pltpu.VMEM((segments, PAD_ROWS + LEN, LANES), F32),
            pltpu.VMEM((group_rows, LANES), F32),
            pltpu.VMEM((tp, 8, pl.cdiv(group_rows, LANES) * LANES), F32),
            pltpu.VMEM((rows, width), F32),
            pltpu.VMEM((segments, FPAD + LEN, PAIR), F32),
            pltpu.VMEM((pieces, group_rows, LANES), BF16),
            dma((2 + 2 * pieces,)),
            dma((streams, 2)),
            dma((streams, 2, steps)),
            dma((2, 17)),
            dma((2, 17)),
            dma((tp - 1,)),
            dma((tp - 1,)),
        ],
        compiler_params=pltpu.CompilerParams(
            collective_id=0, has_side_effects=True, vmem_limit_bytes=60 * 1024 * 1024
        ),
    )(*args)


def solution(mesh):
    return jax.shard_map(
        shards,
        mesh=mesh,
        in_specs=(
            P(("grp", "fs", "tp"), None),
            P(),
            P("fs", "tp"),
            P("fs", "tp"),
            P(),
            P(),
            P("tp", "fs"),
            P(),
            P(),
            P("fs", "tp"),
            P("fs", "tp"),
            P(),
            P("tp", "fs"),
            P(),
        ),
        out_specs=P(("grp", "fs", "tp"), None),
        check_vma=False,
    )
```

time: 473 us -> 245 us (0.52)
  waiting for transfers between devices: 280 us -> 0 us
  Pallas kernels: 0 us -> 234 us
  starting transfers between devices: 105 us -> 0 us
  blocking collectives: 46.8 us -> 0 us
  between operations: 13.3 us -> 0.02 us
  matrix products: 12.1 us -> 0 us
  other arithmetic: 11.8 us -> 0 us
  local copies, waits for them, and re-layouts: 3.54 us -> 11.1 us
    pallas_call x0 -> x1, Pallas kernels: none -> 234 us  [shards(): pl.pallas_call(functools.partial(layer_kernel, n, tp), out_shape=jax.Shap...]
    all_gather x3 -> x0, waiting for transfers between devices: 224 us -> none  [the longest x1 125 us: shards(): down_full = lax.all_gather(down_weight, 'fs', axis=1, tiled=True)]
    all_to_all x5 -> x0, starting transfers between devices: 105 us -> none  [the longest x3 74.9 us: from_everyone(): return lax.all_to_all(copies, axis, split_axis=0, concat_axis=0, tiled=True)]
    all_to_all x5 -> x0, waiting for transfers between devices: 55.7 us -> none  [the longest x2 34.8 us: summed_on_arrival(): lax.all_to_all(blocks, axis, split_axis=0, concat_axis=0, tiled=True)]
    all_gather x1 -> x0, blocking collectives: 46.8 us -> none  [shards(): out_full = lax.all_gather(out_weight, 'fs', axis=1, tiled=True)]
    dot_general x6 -> x0, matrix products: 12.1 us -> none  [the longest x2 5.69 us: make_rows_product(): return jnp.dot(left, weight, preferred_element_type=jnp.float32)]
    reshape x0 -> x5, local copies, waits for them, and re-layouts: none -> 6.42 us  [shards(): args = [a.reshape(1, -1) if a.ndim == 1 else a for a in args]]
    convert_element_type x12 -> x0, other arithmetic: 5.42 us -> none  [the longest x2 1.55 us: depthwise(): tap_values = tap_table.astype(jnp.float32)]
  transfers between devices with their start and end apart: 8 -> 0, of which waited for: 7 -> 0; matrix products, arithmetic and copies ran while one was open for 4% -> 0% of each run, Pallas kernels for 0% -> 0%
where the time goes in v1:
time: 245 us
  Pallas kernels  234 us (96%)
  local copies, waits for them, and re-layouts  11.1 us (5%)
    pallas_call x1, Pallas kernels, shards(): pl.pallas_call(functools.partial(layer_kernel, n, tp), out_shape=jax.Shap...  234 us
    reshape x5, local copies, waits for them, and re-layouts, shards(): args = [a.reshape(1, -1) if a.ndim == 1 else a for a in args]  6.42 us

profile of v1, /device:TPU:33, one launch (start us, length us, event | category | flops | bytes accessed | tf_op | source)
XLA Modules:
  0.0 244.8 jit_solution(7807847111288505149)
XLA Ops:
  0.0 0.0 copy-start.1
  0.0 1.3 reshape.16.chan_gain
  1.3 1.3 reshape.15.mix_gain
  2.6 1.3 reshape.17.mix_post_gain
  3.9 1.3 reshape.18.ffn_gain
  5.1 1.3 reshape.19.ffn_post_gain
  6.4 1.4 copy.15.out_w
  7.8 0.0 copy-done.1
  7.9 0.0 copy-start
  7.9 0.7 copy.16.ffn_taps
  8.5 0.2 copy-done
  8.7 0.8 copy.17.down_w
  9.5 233.6 %shard_map.136 = bf16[40,2048]{1,0:T(8,128)(2,1)} custom-call(bf16[40,2048]{1,0:T(8,128)(2,1)} %tokens.1, bf16[1,2048]{1,0:T(2,128)(2,1)} %reshape.15.mix_gain, bf16[64,128]{1,0:T(8,128)(2,1)} %val_h.1, bf16[64,128]{1,0:T(8,128)(2,1)} %gate_h.1, bf16[31,1024]{1,0:T(8,128)(2,1)} %conv_taps.1, bf16[1,1024]{1,0:T(2,128)(2,1)} %reshape.16.chan_gain, ...), custom_call_target="tpu_custom_call" | custom-call | tf_op jit(solution)/shard_map/pallas_call | solution.py:541
  243.2 1.6 copy.19
Async XLA Ops:
  0.0 7.9 %copy-start.1 = (bf16[2,3,5120]{2,0,1:T(2,128)(2,1)S(1)}, bf16[2,3,5120]{2,0,1:T(2,128)(2,1)}, u32[]{:S(2)}) copy-start(bf16[2,3,5120]{2,0,1:T(2,128)(2,1)} %param.25) | copy-start | bytes 184324
  7.9 0.9 copy-start

commit v2 on v1

--- a/solution.py
+++ b/solution.py
@@ -19,18 +19,19 @@
 LANES = 128
 PAIR = 2 * LANES
 PAD_ROWS = 32
+LATE = 0
 FPAD = 8
 
 
 class Ring:
-    def __init__(self, n, me, block, streams, offsets, send_sem, recv_sem):
-        self.n, self.me, self.block = n, me, block
-        self.streams, self.offsets = streams, offsets
-        self.send_sem, self.recv_sem = send_sem, recv_sem
+    def __init__(self, n, me, streams, offsets, shared, mate, sems):
+        self.n, self.me = n, me
+        self.streams, self.offsets, self.shared, self.mate = streams, offsets, shared, mate
+        self.send_sem, self.recv_sem, self.ysend, self.yrecv = sems
         self.steps = (n // 2, (n - 1) - n // 2)
         self.peers = (lax.rem(me + 1, n), lax.rem(me + n - 1, n))
         self.at = 0
-        self.last = max(offsets) + self.steps[0]
+        self.last = max(offsets) + self.steps[0] + 1
 
     def copy(self, j, way, owner, step):
         ref = self.streams[j](owner)
@@ -43,72 +44,77 @@
             device_id_type=MESH,
         )
 
+    def across(self, j, owner):
+        if j in self.shared:
+            ref = self.streams[j](owner)
+            pltpu.make_async_remote_copy(
+                src_ref=ref,
+                dst_ref=ref,
+                send_sem=self.ysend.at[j],
+                recv_sem=self.yrecv.at[j],
+                device_id={"grp": self.mate},
+                device_id_type=MESH,
+            ).start()
+
     def owner(self, way, step):
         shift = (self.n - step) if way == 0 else step
         return lax.rem(self.me + shift, self.n)
 
-    def arrived(self, j, way, step):
-        self.copy(j, way, self.owner(way, step + 1), step).wait_recv()
-
-    def slot(self, k, active):
-        for j, first in active:
+    def step(self, j, way, step, forward):
+        owner = self.owner(way, step)
+        self.copy(j, way, owner, step - 1).wait_recv()
+        if forward:
+            self.copy(j, way, owner, step).start()
+        self.across(j, owner)
+
+    def slot(self, k):
+        for j, off in enumerate(self.offsets):
             for way in (0, 1):
-                step = k - self.offsets[j]
-                if first:
+                step = k - off
+                if step == 0:
                     if self.steps[way] > 0:
                         self.copy(j, way, self.me, 0).start()
-                    continue
-
-                def go(j=j, way=way, step=step):
-                    self.arrived(j, way, step - 1)
-                    self.copy(j, way, self.owner(way, step), step).start()
-
-                if way == 0 or isinstance(step, int):
-                    if step < self.steps[way] if isinstance(step, int) else True:
-                        go()
-                else:
-                    pl.when(step < self.steps[way])(go)
-
-    def active(self, k):
-        return tuple(
-            (j, k == off)
-            for j, off in enumerate(self.offsets)
-            if off <= k < off + self.steps[0]
-        )
-
-    def short(self, k):
-        return tuple(k - off >= self.steps[1] for off in self.offsets)
+                elif 0 < step <= self.steps[way]:
+                    self.step(j, way, step, step < self.steps[way])
+
+    def slot_loop(self, k, active):
+        for j in active:
+            for way in (0, 1):
+                self.step(j, way, k - self.offsets[j], True)
+
+    def kinds(self, k):
+        passing, other = [], False
+        for j, off in enumerate(self.offsets):
+            step = k - off
+            if 0 < step < self.steps[1]:
+                passing.append(j)
+            elif 0 <= step <= self.steps[0]:
+                other = True
+        return tuple(passing), other
 
     def pump_to(self, upto):
         upto = min(upto, self.last)
         while self.at < upto:
-            key = (self.active(self.at), self.short(self.at))
-            end = self.at
-            while end < upto and (self.active(end), self.short(end)) == key:
+            kinds = self.kinds(self.at)
+            end = self.at + 1
+            while end < upto and not kinds[1] and self.kinds(end) == kinds:
                 end += 1
-            steady = end - self.at > 1 and not any(f for _, f in key[0])
-            if steady and not any(key[1][j] for j, _ in key[0]):
+            if end - self.at > 1:
                 lax.fori_loop(
-                    self.at, end, lambda k, z, key=key: (self.slot_loop(k, key[0]), z)[1], 0
+                    self.at, end, lambda k, z, on=kinds[0]: (self.slot_loop(k, on), z)[1], 0
                 )
-                self.at = end
             else:
-                self.slot(self.at, self.active(self.at))
-                self.at += 1
-
-    def slot_loop(self, k, active):
-        for j, _ in active:
-            for way in (0, 1):
-                step = k - self.offsets[j]
-                self.arrived(j, way, step - 1)
-                self.copy(j, way, self.owner(way, step), step).start()
+                self.slot(self.at)
+            self.at = end
+
+    def pump(self, count=1):
+        self.pump_to(self.at + count)
 
     def finish(self, js):
-        self.pump_to(max(self.offsets[j] + self.steps[0] for j in js))
-        for j in js:
-            for way in (0, 1):
-                if self.steps[way] > 0:
-                    self.arrived(j, way, self.steps[way] - 1)
+        self.pump_to(max(self.offsets[j] for j in js) + self.steps[0] + 1)
+
+    def handed(self, j, whole):
+        pltpu.make_async_copy(whole, whole, self.yrecv.at[j]).wait()
 
     def drain(self, wholes):
         for j, whole in enumerate(wholes):
@@ -116,6 +122,9 @@
                 if self.steps[way] > 0:
                     ref = whole(self.steps[way])
                     pltpu.make_async_copy(ref, ref, self.send_sem.at[j, way]).wait()
+            if j in self.shared:
+                ref = whole(self.n - 1)
+                pltpu.make_async_copy(ref, ref, self.ysend.at[j]).wait()
 
 
 def layer_kernel(
@@ -127,13 +136,13 @@
     gate_h,
     conv_taps,
     chan_gain,
-    out_w,
+    out_h,
     mix_post_gain,
     ffn_gain,
     up_gate_h,
     up_val_h,
     ffn_taps,
-    down_w,
+    down_h,
     ffn_post_gain,
     out,
     vg,
@@ -156,9 +165,12 @@
     resid,
     fbuf,
     hidden,
+    cgain,
     load_sem,
     zsend,
     zrecv,
+    ysend,
+    yrecv,
     xsend,
     xrecv,
     ssend,
@@ -178,6 +190,9 @@
     xr, xl, xo = (lax.rem(x + s, chips) for s in (1, chips - 1, 2))
     tr, tl, to = (2 * v + c for v in (xr, xl, xo))
     odd = c == 1
+    g = lax.axis_index("grp")
+    side = lax.rem(g, 2)
+    mate = g + 1 - 2 * side
 
     mine = pl.ds(pl.multiple_of(f * block, block), block)
     loads = [
@@ -196,6 +211,8 @@
                 up_val_h.at[:, columns], up.at[j, mine, pl.ds(LANES, LANES)], load_sem.at[3 + 2 * j]
             )
         )
+    loads.append(pltpu.make_async_copy(out_h, outt.at[mine, :], load_sem.at[2 + 2 * pieces]))
+    loads.append(pltpu.make_async_copy(down_h, downt.at[mine, :], load_sem.at[3 + 2 * pieces]))
     for load in loads:
         load.start()
 
@@ -207,14 +224,7 @@
             barrier, inc=1, device_id={"tp": lax.rem(t + d, tp)}, device_id_type=MESH
         )
 
-    eye = jnp.where(
-        lax.broadcasted_iota(jnp.int32, (block, block), 0)
-        == lax.broadcasted_iota(jnp.int32, (block, block), 1),
-        1.0,
-        0.0,
-    ).astype(BF16)
-    outt[mine, :] = lax.dot_general(eye, out_w[...], NT, preferred_element_type=F32).astype(BF16)
-    downt[mine, :] = lax.dot_general(eye, down_w[...], NT, preferred_element_type=F32).astype(BF16)
+    pl.semaphore_signal(barrier, inc=1, device_id={"grp": mate}, device_id_type=MESH)
 
     def zview(buffer, owner):
         return buffer.at[pl.ds(pl.multiple_of(owner * block, block), block), :]
@@ -224,14 +234,19 @@
         start = pl.multiple_of(owner * block + part * size, size)
         return downt.at[pl.ds(start, size), :]
 
+    share = pieces // 2
+    own = [side * share + i for i in range(share)]
+    far = [(1 - side) * share + i for i in range(share)]
+    both_sides = list(range(2 * share, pieces))
     streams = [functools.partial(zview, vg), functools.partial(zview, outt)]
-    streams += [functools.partial(zview, up.at[j]) for j in range(pieces)]
-    streams += [functools.partial(down_view, part) for part in (0, 1)]
-    steps = n // 2
-    ups = list(range(2, 2 + pieces))
-    downs = [2 + pieces, 3 + pieces]
-    offsets = [0, 0] + [0 if j < 2 else steps for j in range(pieces)] + [2 * steps] * 2
-    ring = Ring(n, f, block, streams, offsets, zsend, zrecv)
+    streams += [functools.partial(zview, up.at[j]) for j in own]
+    streams += [functools.partial(down_view, side)]
+    streams += [functools.partial(zview, up.at[j]) for j in both_sides]
+    own_at = list(range(2, 2 + share))
+    down_at = 2 + share
+    both_at = list(range(down_at + 1, len(streams)))
+    offsets = [0, 0] + [0] * share + [min(LATE, n // 2)] * (1 + len(both_sides))
+    ring = Ring(n, f, streams, offsets, own_at + [down_at], mate, (zsend, zrecv, ysend, yrecv))
 
     def put_normed(u, left, right, gain):
         scale = lax.rsqrt(
@@ -244,7 +259,7 @@
         )
         pad = jnp.zeros((8, half), F32)
         for at, part in ((0, left), (half, right)):
-            value = part * scale * gain[:, at : at + half].astype(F32)
+            value = part * scale * gain[at : at + half].astype(F32).reshape(1, half)
             low = jnp.concatenate([value, pad], axis=0)
             high = jnp.concatenate([pad, value], axis=0)
             xg[u, t, :, at : at + half] = jnp.where(odd, high, low).astype(BF16)
@@ -364,13 +379,15 @@
     left = tokens[:, 0:half].astype(F32)
     right = tokens[:, half:width].astype(F32)
     put_normed(0, left, right, mix_gain)
-    pl.semaphore_wait(barrier, tp + 1)
+    cgain[...] = chan_gain[...].astype(F32).reshape(1, -1)
+    pl.semaphore_wait(barrier, tp + 2)
     for load in loads:
         load.wait()
     ring.pump_to(1)
     sent = spread(0, (2, 4, 5))
 
     ring.finish([0])
+    ring.pump()
     both = jnp.dot(lhs[...], vg[...], preferred_element_type=F32)
     glu = (both[:, 0:LANES] * jax.nn.sigmoid(both[:, LANES:PAIR])).astype(BF16).astype(F32)
     segments = group_rows // LEN
@@ -391,6 +408,7 @@
 
     lax.fori_loop(0, segments, convolve, 0)
     conv_out = conv[...]
+    ring.pump()
     ones = jnp.ones((8, LANES), F32)
     high = lax.Precision.HIGHEST
     sums = lax.dot_general(ones, conv_out, NT, precision=high, preferred_element_type=F32)
@@ -413,7 +431,7 @@
     stat_copies = [stat_copy(d) for d in range(1, tp)]
     for copy in stat_copies:
         copy.start()
-    ring.finish([1])
+    ring.pump()
     for d in range(1, tp):
         source = lax.rem(t + tp - d, tp)
         pltpu.make_async_remote_copy(
@@ -424,14 +442,14 @@
             device_id={"tp": source},
             device_id_type=MESH,
         ).wait_recv()
-    channels = chan_gain.shape[1]
+    channels = chan_gain.shape[0]
     both_stats = jnp.sum(stats[:, :, 0:group_rows], axis=0) / channels
     flipped = jnp.transpose(
         jnp.concatenate([both_stats] + [jnp.zeros((8, group_rows), F32)] * 15, axis=0)
     )
     mean, square = flipped[:, 0:1], flipped[:, 4:5]
     scale = lax.rsqrt(square - mean * mean + chan_epsilon)
-    normal = (conv_out - mean) * scale * chan_gain[:, my_ch].astype(F32)
+    normal = (conv_out - mean) * scale * cgain[:, my_ch]
     activated = (normal * jax.nn.sigmoid(normal)).astype(BF16)
     wide = min(512, width)
     for j in range(width // wide):
@@ -439,8 +457,9 @@
             activated, outt[j * wide : (j + 1) * wide, :], NT, preferred_element_type=F32
         ).astype(BF16)
 
+    ring.pump()
     base = ring.at
-    left_sum, right_sum, more = collect(0, (base + 1, base + 2, base + 4, base + 5))
+    left_sum, right_sum, more = collect(0, (base + 1, base + 3, base + 5, base + 6))
     sent += more
 
     def rms(a, b, gain):
@@ -449,8 +468,8 @@
             + norm_epsilon
         )
         return (
-            a * scale * gain[:, 0:half].astype(F32),
-            b * scale * gain[:, half:width].astype(F32),
+            a * scale * gain[0:half].astype(F32).reshape(1, half),
+            b * scale * gain[half:width].astype(F32).reshape(1, half),
         )
 
     a, b = rms(left_sum, right_sum, mix_post_gain)
@@ -461,17 +480,18 @@
     put_normed(1, res_a.astype(F32), res_b.astype(F32), ffn_gain)
     base = ring.at
     sent += spread(1, (base + 1, base + 2, base + 3))
+    ring.pump_to(ring.last)
 
     fbuf[:, 0:FPAD, :] = jnp.zeros((segments, FPAD, PAIR), F32)
-    ftaps_n = ffn_taps.shape[1]
+    ftaps_n = ffn_taps.shape[0]
 
     def feed(j):
         pair = jnp.dot(lhs[...], up[j], preferred_element_type=F32).astype(BF16).astype(F32)
         for s in range(segments):
             fbuf[s, FPAD:, :] = pair[s * LEN : (s + 1) * LEN, :]
         here = pl.ds(pl.multiple_of(t * (pieces * LANES) + j * LANES, LANES), LANES)
-        gate_taps = ffn_taps[0, :, here].astype(F32)
-        val_taps = ffn_taps[1, :, here].astype(F32)
+        gate_taps = ffn_taps[:, 0, here].astype(F32)
+        val_taps = ffn_taps[:, 1, here].astype(F32)
         for s in range(segments):
             gate = jnp.zeros((LEN, LANES), F32)
             val = jnp.zeros((LEN, LANES), F32)
@@ -483,17 +503,12 @@
                 jax.nn.gelu(gate, approximate=True) * val
             ).astype(BF16)
 
-    early = [j for j in range(pieces) if offsets[2 + j] == 0]
-    late = [j for j in range(pieces) if offsets[2 + j] > 0]
-    ring.finish([2 + j for j in early])
-    for j in early:
+    for j in own + both_sides:
         feed(j)
-        ring.pump_to(ring.at + 1)
-    ring.finish([2 + j for j in late])
-    for j in late:
+    for at, j in zip(own_at, far):
+        ring.handed(at, up.at[j, 0 : (n - 1) * block, :])
         feed(j)
-        ring.pump_to(ring.at + 2)
-    ring.finish(downs)
+    ring.handed(down_at, downt.at[0 : (n - 1) * (block // 2), :])
 
     def contract(j, z):
         columns = pl.ds(pl.multiple_of(j * PAIR, PAIR), PAIR)
@@ -517,31 +532,31 @@
         return buffer.at[pl.ds(0, count * size), :]
 
     wholes = [functools.partial(whole_of, vg, block), functools.partial(whole_of, outt, block)]
-    wholes += [functools.partial(whole_of, up.at[j], block) for j in range(pieces)]
-    wholes += [functools.partial(whole_of, downt, block // 2)] * 2
+    wholes += [functools.partial(whole_of, up.at[0], block)] * share
+    wholes += [functools.partial(whole_of, downt, block // 2)]
+    wholes += [functools.partial(whole_of, up.at[0], block)] * len(both_sides)
     ring.drain(wholes)
 
 
 def shards(*args):
-    (tokens, mix_gain, val_weight, _, conv_taps, chan_gain, out_weight) = args[:7]
-    up_weight, down_weight = args[9], args[12]
+    tokens, up_weight = args[0], args[9]
     n, tp = lax.axis_size("fs"), lax.axis_size("tp")
     rows, width = tokens.shape
-    block = width // n
     half, quarter = width // 2, width // 4
     group_rows, chip_rows = rows * tp, 2 * rows
     segments = group_rows // LEN
     pieces = up_weight.shape[1] // LANES
-    streams = 4 + pieces
+    streams = 3 + pieces - pieces // 2
     steps = n // 2
-    args = [a.reshape(1, -1) if a.ndim == 1 else a for a in args]
+    args = list(args)
+    args[6], args[12], args[11] = args[6].T, args[12].T, args[11].transpose(1, 0, 2)
     vmem = pl.BlockSpec(memory_space=pltpu.VMEM)
     hbm = pl.BlockSpec(memory_space=pltpu.HBM)
     dma = pltpu.SemaphoreType.DMA
     return pl.pallas_call(
         functools.partial(layer_kernel, n, tp),
         out_shape=jax.ShapeDtypeStruct((rows, width), BF16),
-        in_specs=[hbm if i in (2, 3, 9, 10) else vmem for i in range(len(args))],
+        in_specs=[hbm if i in (2, 3, 6, 9, 10, 12) else vmem for i in range(len(args))],
         out_specs=vmem,
         scratch_shapes=[
             pltpu.VMEM((width, PAIR), BF16),
@@ -564,9 +579,12 @@
             pltpu.VMEM((rows, width), F32),
             pltpu.VMEM((segments, FPAD + LEN, PAIR), F32),
             pltpu.VMEM((pieces, group_rows, LANES), BF16),
-            dma((2 + 2 * pieces,)),
+            pltpu.VMEM((1, args[5].shape[0]), F32),
+            dma((4 + 2 * pieces,)),
             dma((streams, 2)),
             dma((streams, 2, steps)),
+            dma((streams,)),
+            dma((streams,)),
             dma((2, 17)),
             dma((2, 17)),
             dma((tp - 1,)),

time: 245 us -> 169 us (0.69)
  Pallas kernels: 234 us -> 167 us
  local copies, waits for them, and re-layouts: 11.1 us -> 1.59 us
    pallas_call x1, Pallas kernels: 234 us -> 167 us  [shards(): pl.pallas_call(functools.partial(layer_kernel, n, tp), out_shape=jax.Shap...]
    reshape x5 -> x0, local copies, waits for them, and re-layouts: 6.42 us -> none  [shards(): args = [a.reshape(1, -1) if a.ndim == 1 else a for a in args]]
    unnamed x8 -> x1, local copies, waits for them, and re-layouts: 4.71 us -> 1.59 us
where the time goes in v2:
time: 169 us; the launch traced here: 168 us
  Pallas kernels  167 us (99%)
    pallas_call x1, Pallas kernels, shards(): pl.pallas_call(functools.partial(layer_kernel, n, tp), out_shape=jax.Shap...  167 us

profile of v2, /device:TPU:33, one launch (start us, length us, event | category | flops | bytes accessed | tf_op | source)
XLA Modules:
  0.0 168.3 jit_solution(14941695347913536342)
XLA Ops:
  0.0 166.7 %shard_map.136 = bf16[40,2048]{1,0:T(8,128)(2,1)} custom-call(bf16[40,2048]{1,0:T(8,128)(2,1)} %tokens.1, bf16[2048]{0:T(1024)(128)(2,1)} %mix_gain.1, bf16[64,128]{1,0:T(8,128)(2,1)} %val_h.1, bf16[64,128]{1,0:T(8,128)(2,1)} %gate_h.1, bf16[31,1024]{1,0:T(8,128)(2,1)} %conv_taps.1, bf16[1024]{0:T(1024)(128)(2,1)} %chan_gain.1, bf16[64,128]{1,0:T(8,128)(2,1)} %bitcast.5, ...), custom_call_target="tpu_custom_call" | custom-call | tf_op jit(solution)/shard_map/pallas_call | solution.py:556
  166.8 1.6 copy.16

commit v3 on v2

--- a/solution.py
+++ b/solution.py
@@ -24,23 +24,30 @@
 
 
 class Ring:
-    def __init__(self, n, me, streams, offsets, shared, mate, sems):
+    def __init__(self, n, me, streams, offsets, strides, shared, mate, sems):
         self.n, self.me = n, me
-        self.streams, self.offsets, self.shared, self.mate = streams, offsets, shared, mate
+        self.streams, self.offsets, self.strides = streams, offsets, strides
+        self.shared, self.mate = shared, mate
         self.send_sem, self.recv_sem, self.ysend, self.yrecv = sems
-        self.steps = (n // 2, (n - 1) - n // 2)
-        self.peers = (lax.rem(me + 1, n), lax.rem(me + n - 1, n))
+        self.reach = (n // 2, (n - 1) - n // 2)
         self.at = 0
-        self.last = max(offsets) + self.steps[0] + 1
-
-    def copy(self, j, way, owner, step):
+        self.last = max(self.end(j) for j in range(len(streams)))
+
+    def end(self, j):
+        return self.offsets[j] + pl.cdiv(self.reach[0], self.strides[j]) + 1
+
+    def place(self, way, distance):
+        shift = distance if way == 0 else self.n - distance
+        return lax.rem(self.me + shift, self.n)
+
+    def copy(self, j, way, owner, hop, distance):
         ref = self.streams[j](owner)
         return pltpu.make_async_remote_copy(
             src_ref=ref,
             dst_ref=ref,
             send_sem=self.send_sem.at[j, way],
-            recv_sem=self.recv_sem.at[j, way, step],
-            device_id={"fs": self.peers[way]},
+            recv_sem=self.recv_sem.at[j, way, distance - 1],
+            device_id={"fs": self.place(way, hop)},
             device_id_type=MESH,
         )
 
@@ -56,39 +63,41 @@
                 device_id_type=MESH,
             ).start()
 
-    def owner(self, way, step):
-        shift = (self.n - step) if way == 0 else step
-        return lax.rem(self.me + shift, self.n)
-
-    def step(self, j, way, step, forward):
-        owner = self.owner(way, step)
-        self.copy(j, way, owner, step - 1).wait_recv()
+    def step(self, j, way, distance, forward):
+        hop = self.strides[j]
+        owner = self.place(1 - way, distance)
+        self.copy(j, way, owner, hop, distance).wait_recv()
         if forward:
-            self.copy(j, way, owner, step).start()
+            self.copy(j, way, owner, hop, distance + hop).start()
         self.across(j, owner)
 
     def slot(self, k):
         for j, off in enumerate(self.offsets):
+            hop, turn = self.strides[j], k - off
             for way in (0, 1):
-                step = k - off
-                if step == 0:
-                    if self.steps[way] > 0:
-                        self.copy(j, way, self.me, 0).start()
-                elif 0 < step <= self.steps[way]:
-                    self.step(j, way, step, step < self.steps[way])
+                if turn == 0:
+                    for far in range(1, min(hop, self.reach[way]) + 1):
+                        self.copy(j, way, self.me, far, far).start()
+            for i in range(1, hop + 1):
+                for way in (0, 1):
+                    distance = (turn - 1) * hop + i
+                    if turn > 0 and distance <= self.reach[way]:
+                        self.step(j, way, distance, distance + hop <= self.reach[way])
 
     def slot_loop(self, k, active):
         for j in active:
-            for way in (0, 1):
-                self.step(j, way, k - self.offsets[j], True)
+            hop = self.strides[j]
+            for i in range(1, hop + 1):
+                for way in (0, 1):
+                    self.step(j, way, (k - self.offsets[j] - 1) * hop + i, True)
 
     def kinds(self, k):
         passing, other = [], False
         for j, off in enumerate(self.offsets):
-            step = k - off
-            if 0 < step < self.steps[1]:
+            turn = k - off
+            if turn > 0 and (turn + 1) * self.strides[j] <= self.reach[1]:
                 passing.append(j)
-            elif 0 <= step <= self.steps[0]:
+            elif 0 <= turn and k < self.end(j):
                 other = True
         return tuple(passing), other
 
@@ -111,7 +120,7 @@
         self.pump_to(self.at + count)
 
     def finish(self, js):
-        self.pump_to(max(self.offsets[j] for j in js) + self.steps[0] + 1)
+        self.pump_to(max(self.end(j) for j in js))
 
     def handed(self, j, whole):
         pltpu.make_async_copy(whole, whole, self.yrecv.at[j]).wait()
@@ -119,8 +128,8 @@
     def drain(self, wholes):
         for j, whole in enumerate(wholes):
             for way in (0, 1):
-                if self.steps[way] > 0:
-                    ref = whole(self.steps[way])
+                if self.reach[way] > 0:
+                    ref = whole(self.reach[way])
                     pltpu.make_async_copy(ref, ref, self.send_sem.at[j, way]).wait()
             if j in self.shared:
                 ref = whole(self.n - 1)
@@ -217,8 +226,8 @@
         load.start()
 
     barrier = pltpu.get_barrier_semaphore()
-    for z in (lax.rem(f + 1, n), lax.rem(f + n - 1, n)):
-        pl.semaphore_signal(barrier, inc=1, device_id={"fs": z}, device_id_type=MESH)
+    for z in (1, 2, n - 2, n - 1):
+        pl.semaphore_signal(barrier, inc=1, device_id={"fs": lax.rem(f + z, n)}, device_id_type=MESH)
     for d in range(1, tp):
         pl.semaphore_signal(
             barrier, inc=1, device_id={"tp": lax.rem(t + d, tp)}, device_id_type=MESH
@@ -245,8 +254,9 @@
     own_at = list(range(2, 2 + share))
     down_at = 2 + share
     both_at = list(range(down_at + 1, len(streams)))
-    offsets = [0, 0] + [0] * share + [min(LATE, n // 2)] * (1 + len(both_sides))
-    ring = Ring(n, f, streams, offsets, own_at + [down_at], mate, (zsend, zrecv, ysend, yrecv))
+    offsets = [0, min(3, n // 2)] + [0] * share + [min(LATE, n // 2)] * (1 + len(both_sides))
+    strides = [2, 2] + [1] * (len(streams) - 2)
+    ring = Ring(n, f, streams, offsets, strides, own_at + [down_at], mate, (zsend, zrecv, ysend, yrecv))
 
     def put_normed(u, left, right, gain):
         scale = lax.rsqrt(
@@ -328,11 +338,27 @@
 
     q0, q1 = pl.ds(0, quarter), pl.ds(quarter, quarter)
 
-    def collect(u, slots):
-        mine_h = pl.ds(pl.multiple_of(c * half, half), half)
-        other_h = pl.ds(pl.multiple_of((1 - c) * half, half), half)
-        sent = [x_copy(u, 9, prod.at[u, :, other_h], din.at[u], partner)]
-        sent[0].start()
+    mine_h = pl.ds(pl.multiple_of(c * half, half), half)
+    other_h = pl.ds(pl.multiple_of((1 - c) * half, half), half)
+
+    def multiply(u, left, weight, wide):
+        sent = x_copy(u, 9, prod.at[u, :, other_h], din.at[u], partner)
+        for side_at in (1 - c, c):
+
+            def piece(j, z, side_at=side_at):
+                columns = pl.ds(pl.multiple_of(side_at * half + j * wide, wide), wide)
+                prod[u, :, columns] = lax.dot_general(
+                    left, weight[columns, :], NT, preferred_element_type=F32
+                ).astype(BF16)
+                return z
+
+            lax.fori_loop(0, half // wide, piece, 0)
+            if side_at is not c:
+                sent.start()
+        return sent
+
+    def collect(u, handed, slots):
+        sent = [handed]
         ring.pump_to(slots[0])
         x_copy(u, 9, prod.at[u, :, other_h], din.at[u], partner).wait_recv()
         psum[u, :, :] = (
@@ -380,11 +406,11 @@
     right = tokens[:, half:width].astype(F32)
     put_normed(0, left, right, mix_gain)
     cgain[...] = chan_gain[...].astype(F32).reshape(1, -1)
-    pl.semaphore_wait(barrier, tp + 2)
+    pl.semaphore_wait(barrier, tp + 4)
     for load in loads:
         load.wait()
     ring.pump_to(1)
-    sent = spread(0, (2, 4, 5))
+    sent = spread(0, (3, 4, 5))
 
     ring.finish([0])
     ring.pump()
@@ -408,7 +434,7 @@
 
     lax.fori_loop(0, segments, convolve, 0)
     conv_out = conv[...]
-    ring.pump()
+    ring.pump(1)
     ones = jnp.ones((8, LANES), F32)
     high = lax.Precision.HIGHEST
     sums = lax.dot_general(ones, conv_out, NT, precision=high, preferred_element_type=F32)
@@ -431,7 +457,7 @@
     stat_copies = [stat_copy(d) for d in range(1, tp)]
     for copy in stat_copies:
         copy.start()
-    ring.pump()
+    ring.pump(0)
     for d in range(1, tp):
         source = lax.rem(t + tp - d, tp)
         pltpu.make_async_remote_copy(
@@ -451,15 +477,11 @@
     scale = lax.rsqrt(square - mean * mean + chan_epsilon)
     normal = (conv_out - mean) * scale * cgain[:, my_ch]
     activated = (normal * jax.nn.sigmoid(normal)).astype(BF16)
-    wide = min(512, width)
-    for j in range(width // wide):
-        prod[0, :, j * wide : (j + 1) * wide] = lax.dot_general(
-            activated, outt[j * wide : (j + 1) * wide, :], NT, preferred_element_type=F32
-        ).astype(BF16)
-
-    ring.pump()
+    ring.finish([1])
+    handed = multiply(0, activated, outt, min(512, half))
+    ring.pump(1)
     base = ring.at
-    left_sum, right_sum, more = collect(0, (base + 1, base + 3, base + 5, base + 6))
+    left_sum, right_sum, more = collect(0, handed, (base + 0, base + 1, base + 1, base + 2))
     sent += more
 
     def rms(a, b, gain):
@@ -479,8 +501,7 @@
     resid[:, half:width] = res_b.astype(F32)
     put_normed(1, res_a.astype(F32), res_b.astype(F32), ffn_gain)
     base = ring.at
-    sent += spread(1, (base + 1, base + 2, base + 3))
-    ring.pump_to(ring.last)
+    sent += spread(1, (base + 1, base + 2, base + 2))
 
     fbuf[:, 0:FPAD, :] = jnp.zeros((segments, FPAD, PAIR), F32)
     ftaps_n = ffn_taps.shape[0]
@@ -503,23 +524,21 @@
                 jax.nn.gelu(gate, approximate=True) * val
             ).astype(BF16)
 
-    for j in own + both_sides:
+    ring.finish(own_at)
+    for j in own:
+        feed(j)
+        ring.pump()
+    ring.pump_to(ring.last)
+    for j in both_sides:
         feed(j)
     for at, j in zip(own_at, far):
         ring.handed(at, up.at[j, 0 : (n - 1) * block, :])
         feed(j)
     ring.handed(down_at, downt.at[0 : (n - 1) * (block // 2), :])
 
-    def contract(j, z):
-        columns = pl.ds(pl.multiple_of(j * PAIR, PAIR), PAIR)
-        units = jnp.concatenate([hidden[i] for i in range(pieces)], axis=1)
-        prod[1, :, columns] = lax.dot_general(
-            units, downt[columns, :], NT, preferred_element_type=F32
-        ).astype(BF16)
-        return z
-
-    lax.fori_loop(0, width // PAIR, contract, 0)
-    left_sum, right_sum, more = collect(1, (0, 0, 0, 0))
+    units = jnp.concatenate([hidden[i] for i in range(pieces)], axis=1)
+    handed = multiply(1, units, downt, min(PAIR, half))
+    left_sum, right_sum, more = collect(1, handed, (0, 0, 0, 0))
     sent += more
     a, b = rms(left_sum, right_sum, ffn_post_gain)
     out[:, 0:half] = (resid[:, 0:half] + a).astype(BF16)

time: 169 us -> 166 us (0.982)
  Pallas kernels: 167 us -> 164 us
    pallas_call x1, Pallas kernels: 167 us -> 164 us  [shards(): pl.pallas_call(functools.partial(layer_kernel, n, tp), out_shape=jax.Shap...]
where the time goes in v3:
time: 166 us
  Pallas kernels  164 us (99%)
    pallas_call x1, Pallas kernels, shards(): pl.pallas_call(functools.partial(layer_kernel, n, tp), out_shape=jax.Shap...  164 us

profile of v3, /device:TPU:33, one launch (start us, length us, event | category | flops | bytes accessed | tf_op | source)
XLA Modules:
  0.0 165.6 jit_solution(11431423092825618697)
XLA Ops:
  0.0 164.0 %shard_map.136 = bf16[40,2048]{1,0:T(8,128)(2,1)} custom-call(bf16[40,2048]{1,0:T(8,128)(2,1)} %tokens.1, bf16[2048]{0:T(1024)(128)(2,1)} %mix_gain.1, bf16[64,128]{1,0:T(8,128)(2,1)} %val_h.1, bf16[64,128]{1,0:T(8,128)(2,1)} %gate_h.1, bf16[31,1024]{1,0:T(8,128)(2,1)} %conv_taps.1, bf16[1024]{0:T(1024)(128)(2,1)} %chan_gain.1, bf16[64,128]{1,0:T(8,128)(2,1)} %bitcast.5, ...), custom_call_target="tpu_custom_call" | custom-call | tf_op jit(solution)/shard_map/pallas_call | solution.py:575
  164.0 1.6 copy.16

commit v4 on v3

--- a/solution.py
+++ b/solution.py
@@ -361,19 +361,20 @@
         sent = [handed]
         ring.pump_to(slots[0])
         x_copy(u, 9, prod.at[u, :, other_h], din.at[u], partner).wait_recv()
-        psum[u, :, :] = (
-            prod[u, :, mine_h].astype(F32) + din[u, :, :].astype(F32)
-        ).astype(BF16)
-        plan = [
-            (10, psum.at[u, chip_rows_at(xo), q0], opp.at[u, 0], tr),
-            (11, psum.at[u, chip_rows_at(xo), q1], opp.at[u, 1], tl),
-            (12, psum.at[u, chip_rows_at(xr), q1], near.at[u, 0, 1], tr),
-            (13, psum.at[u, chip_rows_at(xl), q0], near.at[u, 1, 0], tl),
-        ]
-        for item in plan:
-            copy = x_copy(u, *item)
-            copy.start()
-            sent.append(copy)
+        for v, items in (
+            (xo, ((10, q0, opp.at[u, 0], tr), (11, q1, opp.at[u, 1], tl))),
+            (xr, ((12, q1, near.at[u, 0, 1], tr),)),
+            (xl, ((13, q0, near.at[u, 1, 0], tl),)),
+            (x, ()),
+        ):
+            here = chip_rows_at(v)
+            psum[u, here, :] = (
+                prod[u, here, mine_h].astype(F32) + din[u, here, :].astype(F32)
+            ).astype(BF16)
+            for sem, q, dst, where in items:
+                copy = x_copy(u, sem, psum.at[u, here, q], dst, where)
+                copy.start()
+                sent.append(copy)
         ring.pump_to(slots[1])
         for way, sem, v, q, where in ((0, 10, xr, q0, tr), (1, 11, xl, q1, tl)):
             x_copy(u, sem, psum.at[u, chip_rows_at(xo), q], opp.at[u, way], where).wait_recv()
@@ -537,7 +538,7 @@
     ring.handed(down_at, downt.at[0 : (n - 1) * (block // 2), :])
 
     units = jnp.concatenate([hidden[i] for i in range(pieces)], axis=1)
-    handed = multiply(1, units, downt, min(PAIR, half))
+    handed = multiply(1, units, downt, min(512, half))
     left_sum, right_sum, more = collect(1, handed, (0, 0, 0, 0))
     sent += more
     a, b = rms(left_sum, right_sum, ffn_post_gain)

time: 166 us -> 165 us (level)
  no operation moved by 1% of the time
where the time goes in v4:
time: 165 us
  Pallas kernels  163 us (99%)
    pallas_call x1, Pallas kernels, shards(): pl.pallas_call(functools.partial(layer_kernel, n, tp), out_shape=jax.Shap...  163 us

profile of v4, /device:TPU:33, one launch (start us, length us, event | category | flops | bytes accessed | tf_op | source)
XLA Modules:
  0.0 165.0 jit_solution(4736337403021992353)
XLA Ops:
  0.0 163.4 %shard_map.136 = bf16[40,2048]{1,0:T(8,128)(2,1)} custom-call(bf16[40,2048]{1,0:T(8,128)(2,1)} %tokens.1, bf16[2048]{0:T(1024)(128)(2,1)} %mix_gain.1, bf16[64,128]{1,0:T(8,128)(2,1)} %val_h.1, bf16[64,128]{1,0:T(8,128)(2,1)} %gate_h.1, bf16[31,1024]{1,0:T(8,128)(2,1)} %conv_taps.1, bf16[1024]{0:T(1024)(128)(2,1)} %chan_gain.1, bf16[64,128]{1,0:T(8,128)(2,1)} %bitcast.5, ...), custom_call_target="tpu_custom_call" | custom-call | tf_op jit(solution)/shard_map/pallas_call | solution.py:576
  163.4 1.6 copy.16
